TPU v7x, 256 devices: a whole 4x4x8 slice. The times are simulated.
256 devices in a mesh: ep: 64 (over z, y, core), tp: 4 (over x).
Axes of the slice: x: 4, y: 4, z: 8, core: 2. Of those that a mesh axis runs over, the one named last changes fastest.
Arguments:
- tokens: bfloat16 [1536, 2048], P('ep'), may hold values from -6 to 6
- norm_attn: float32 [2048], replicated, may hold values from 0.1 to 1.9
- w_query: bfloat16 [2048, 2048], P(None, 'tp'), may hold values from -0.125 to 0.125
- w_key: bfloat16 [2048, 256], P(None, 'tp'), may hold values from -0.125 to 0.125
- w_value: bfloat16 [2048, 256], P(None, 'tp'), may hold values from -0.125 to 0.125
- w_out: bfloat16 [2048, 2048], P('tp'), may hold values from -1 to 1
- head_bias: float32 [32], P('tp'), may hold values from -7 to -3
- key_cache: bfloat16 [1536, 4, 1024, 64], P('ep', 'tp'), may hold values from -6 to 6
- value_cache: bfloat16 [1536, 4, 1024, 64], P('ep', 'tp'), may hold values from -6 to 6
- lengths: int32 [1536], P('ep'), may hold values from 1 to 1024, 786432 in all
- norm_ffn: float32 [2048], replicated, may hold values from 0.1 to 1.9
- w_group: bfloat16 [2048, 4], replicated, may hold values from -0.125 to 0.125
- w_fine: bfloat16 [2048, 64], replicated, may hold values from -0.125 to 0.125
- routes: int32 [1536, 2], P('ep'), may hold values from 0 to 63, as said below
- e_gate: bfloat16 [64, 2048, 512], P('ep', 'tp'), may hold values from -0.125 to 0.125
- e_up: bfloat16 [64, 2048, 512], P('ep', 'tp'), may hold values from -0.125 to 0.125
- e_down: bfloat16 [64, 512, 2048], P('ep', None, 'tp'), may hold values from -1 to 1
- d_gate: bfloat16 [2048, 8192], P('tp', 'ep'), may hold values from -0.125 to 0.125
- d_up: bfloat16 [2048, 8192], P('tp', 'ep'), may hold values from -0.125 to 0.125
- d_down: bfloat16 [8192, 2048], P('ep', 'tp'), may hold values from -0.25 to 0.25
- w_mix: float32 [2048], replicated, may hold values from -0.125 to 0.125
Outputs:
- mixed: bfloat16 [1536, 2048], P('ep', 'tp')
- new_keys: bfloat16 [1536, 4, 64], P('ep', 'tp')
- new_values: bfloat16 [1536, 4, 64], P('ep', 'tp')
Inputs may be any that keep to these rules, and one draw needn't show every extreme that they name: `routes`: the 2 experts of a row are distinct and lie in one group of 16 consecutive experts. Among the rows of one device each expert is named at most 2 times. One group, the same on every device, is named by exactly 16 rows of every device, so that each of its experts is named exactly 2 times by every device.
All inputs are finite; a program needn't handle non-finite values. No bound on the sum of `lengths` on one device may be relied on, other than what follows from the above.
Results may differ from a plain program's by a relative error of at most 0.019.
Values may be sent and summed in bfloat16 or wider, within the bound.
No kernel may reach another device: no remote copies, remote signals or barrier semaphores. Data moves between devices by JAX's collectives and lax.ppermute only.
A program may use at most 128 MiB of HBM per device.

v0:
```python
import jax
import jax.numpy as jnp
from jax import lax
from jax.sharding import Mesh
from jax.sharding import PartitionSpec as P

GROUPS = 4
TOP_K = 2
EP = ("ep_0", "ep_1", "ep_2")
norm_eps = 1e-06
segment_len = 128


def copy_for_each(x, axis):
    devices = lax.axis_size(axis)
    return lax.all_to_all(jnp.broadcast_to(x[None], (devices, *x.shape)), axis, 0, 0, tiled=True)


def over_copies(x, axis):
    everything = copy_for_each(x, axis)
    return jnp.sum(everything.astype(jnp.float32), axis=0)


def in_order(tiles, dim):
    lengths = list(tiles.shape[1:])
    lengths[dim] *= tiles.shape[0]
    return jnp.moveaxis(tiles, 0, dim).reshape(lengths)


def all_blocks(x, axes, sequence):
    tiles = x[None]
    for k in sequence:
        tiles = lax.all_gather(tiles, axes[k], axis=0, tiled=True)
    current = [lax.axis_size(axes[k]) for k in reversed(sequence)]
    tiles = tiles.reshape(*current, *x.shape)
    turned = sorted(range(len(sequence)), key=lambda place: sequence[len(sequence) - 1 - place])
    return tiles.transpose(*turned, *range(len(sequence), tiles.ndim)).reshape(-1, *x.shape)


def whole_of(x, axes, sequence, dim):
    return in_order(all_blocks(x, axes, sequence), dim)


def normed(values, gains):
    wide = values.astype(jnp.float32)
    return wide * lax.rsqrt(jnp.mean(wide * wide, axis=-1, keepdims=True) + norm_eps) * gains


def suffix_sums(terms):
    length = terms.shape[-1]
    pieces = length // segment_len
    shaped = terms.reshape(terms.shape[:-1] + (pieces, segment_len))
    inner = lax.iota(jnp.int32, segment_len)
    later_inner = (inner[:, None] > inner[None, :]).astype(jnp.float32)
    within = jnp.einsum("...ij,jk->...ik", shaped, later_inner, precision=lax.Precision.HIGHEST)
    outer = lax.iota(jnp.int32, pieces)
    later_outer = (outer[:, None] > outer[None, :]).astype(jnp.float32)
    carried = jnp.einsum(
        "...i,ij->...j", jnp.sum(shaped, axis=-1), later_outer, precision=lax.Precision.HIGHEST
    )
    return (within + carried[..., None]).reshape(terms.shape)


def stick_read(queries, keys, values, lengths, bias_table):
    scores = jnp.einsum("bkgd,bksd->bkgs", queries, keys, preferred_element_type=jnp.float32)
    scores = scores * queries.shape[-1] ** (-0.5) + bias_table[None, :, :, None]
    positions = lax.iota(jnp.int32, keys.shape[2])
    inside = (positions[None, :] < lengths[:, None])[:, None, None, :]
    fails = jnp.where(inside, jax.nn.log_sigmoid(-scores), 0.0)
    weights = jnp.where(inside, jnp.exp(jax.nn.log_sigmoid(scores) + suffix_sums(fails)), 0.0)
    result = jnp.einsum(
        "bkgs,bksd->bkgd", weights.astype(jnp.bfloat16), values, preferred_element_type=jnp.float32
    )
    return result.astype(jnp.bfloat16).reshape(queries.shape[0], -1)


def route_weights(group_logits, fine_logits, chosen, per_group):
    group_iota = lax.iota(jnp.int32, group_logits.shape[1])
    own_group = chosen[:, 0] // per_group
    own_logit = jnp.sum(
        jnp.where(group_iota[None, :] == own_group[:, None], group_logits, 0.0), axis=1
    )
    group_share = 1.0 / jnp.sum(jnp.exp(group_logits - own_logit[:, None]), axis=1)
    expert_iota = lax.iota(jnp.int32, fine_logits.shape[1])
    picked = jnp.sum(
        jnp.where(expert_iota[None, None, :] == chosen[:, :, None], fine_logits[:, None, :], 0.0),
        axis=2,
    )
    within = 1.0 / jnp.sum(jnp.exp(picked[:, None, :] - picked[:, :, None]), axis=2)
    return group_share[:, None] * within


def slot_ranks(flat_routes):
    count = flat_routes.shape[0]
    same_expert = flat_routes[:, None] == flat_routes[None, :]
    position = lax.iota(jnp.int32, count)
    earlier = position[None, :] < position[:, None]
    return jnp.sum(same_expert & earlier, axis=1)


def shards(
    tokens,
    norm_attn,
    w_query,
    w_key,
    w_value,
    w_out,
    head_bias,
    key_cache,
    value_cache,
    lengths,
    norm_ffn,
    w_group,
    w_fine,
    routes,
    e_gate,
    e_up,
    e_down,
    d_gate,
    d_up,
    d_down,
    w_mix,
):
    seq_count = tokens.shape[0]
    width_part = d_gate.shape[0]
    dense_units = d_gate.shape[1]
    expert_units = e_gate.shape[2]
    kv_local = key_cache.shape[1]
    head_dim = key_cache.shape[3]
    ep_size = lax.axis_size(EP)
    per_group = ep_size // GROUPS
    capacity = max(2, (seq_count + per_group - 1) // per_group)
    h_first = normed(tokens, norm_attn).astype(jnp.bfloat16)
    queries = jnp.dot(h_first, w_query, preferred_element_type=jnp.float32).astype(jnp.bfloat16)
    new_keys = jnp.dot(h_first, w_key, preferred_element_type=jnp.float32).astype(jnp.bfloat16)
    new_values = jnp.dot(h_first, w_value, preferred_element_type=jnp.float32).astype(jnp.bfloat16)
    grouped = queries.reshape(seq_count, kv_local, -1, head_dim)
    heads_out = stick_read(
        grouped, key_cache, value_cache, lengths, head_bias.reshape(kv_local, -1)
    )
    partial_value = jnp.dot(heads_out, w_out, preferred_element_type=jnp.float32).astype(
        jnp.bfloat16
    )
    attended = over_copies(
        lax.optimization_barrier(partial_value).astype(jnp.float32).astype(jnp.bfloat16), "tp"
    ).astype(jnp.float32)
    resid = tokens.astype(jnp.float32) + attended
    h_second = normed(resid, norm_ffn).astype(jnp.bfloat16)
    column = lax.axis_index("tp") * width_part
    h_slice = lax.dynamic_slice_in_dim(h_second, column, width_part, 1)
    resid_slice = lax.dynamic_slice_in_dim(resid, column, width_part, 1)
    dense_in = jnp.concatenate([d_gate, d_up], axis=1)
    expert_in = jnp.concatenate([e_gate[0], e_up[0]], axis=1)
    group_logits = jnp.dot(h_second, w_group, preferred_element_type=jnp.float32)
    fine_logits = jnp.dot(h_second, w_fine, preferred_element_type=jnp.float32)
    shares = route_weights(group_logits, fine_logits, routes, per_group)
    mix_gate = jax.nn.sigmoid(
        jnp.dot(h_second.astype(jnp.float32), w_mix, precision=lax.Precision.HIGHEST)
    )
    flat_routes = routes.reshape(-1)
    slot_ids = flat_routes * capacity + slot_ranks(flat_routes)
    onehot = (lax.iota(jnp.int32, ep_size * capacity)[:, None] == slot_ids[None, :]).astype(
        jnp.float32
    )
    repeated = jnp.repeat(h_slice, TOP_K, axis=0)
    outbound = jnp.dot(onehot.astype(jnp.bfloat16), repeated, preferred_element_type=jnp.float32)
    outbound = outbound.astype(jnp.bfloat16).reshape(ep_size, capacity, width_part)
    received = lax.all_to_all(outbound, EP, split_axis=0, concat_axis=0, tiled=True)
    flat_rows = received.reshape(-1, width_part)
    pre_act = over_copies(
        jnp.dot(flat_rows, expert_in, preferred_element_type=jnp.float32).astype(jnp.bfloat16), "tp"
    ).astype(jnp.float32)
    hidden = (jax.nn.silu(pre_act[:, :expert_units]) * pre_act[:, expert_units:]).astype(
        jnp.bfloat16
    )
    result = jnp.dot(hidden, e_down[0], preferred_element_type=jnp.float32).astype(jnp.bfloat16)
    returned = lax.all_to_all(
        result.reshape(received.shape), EP, split_axis=0, concat_axis=0, tiled=True
    )
    weighted = onehot * shares.reshape(-1)[None, :]
    moe_rows = jnp.dot(
        weighted.T,
        returned.reshape(-1, width_part).astype(jnp.float32),
        precision=lax.Precision.HIGHEST,
    )
    moe_slice = jnp.sum(moe_rows.reshape(seq_count, TOP_K, width_part), axis=1)
    dense_pre = jnp.dot(
        whole_of(h_slice, EP, (1, 0, 2), 0), dense_in, preferred_element_type=jnp.float32
    )
    dense_pre = over_copies(dense_pre.astype(jnp.bfloat16), "tp").astype(jnp.float32)
    dense_hidden = (jax.nn.silu(dense_pre[:, :dense_units]) * dense_pre[:, dense_units:]).astype(
        jnp.bfloat16
    )
    own_hidden = lax.all_to_all(dense_hidden, EP, split_axis=0, concat_axis=1, tiled=True)
    dense_slice = jnp.dot(
        own_hidden,
        lax.all_gather(d_down, EP, axis=0, tiled=True),
        preferred_element_type=jnp.float32,
    )
    mixed = resid_slice + moe_slice + mix_gate[:, None] * dense_slice
    return (
        mixed.astype(jnp.bfloat16),
        new_keys.reshape(seq_count, kv_local, head_dim),
        new_values.reshape(seq_count, kv_local, head_dim),
    )


def solution(mesh):
    torus = Mesh(mesh.devices.reshape(8, 4, 2, mesh.shape["tp"]), ("ep_0", "ep_1", "ep_2", "tp"))
    placed = (
        P(EP, None),
        P(),
        P(None, "tp"),
        P(None, "tp"),
        P(None, "tp"),
        P("tp", None),
        P("tp"),
        P(EP, "tp", None, None),
        P(EP, "tp", None, None),
        P(EP),
        P(),
        P(),
        P(),
        P(EP, None),
        P(EP, "tp", None),
        P(EP, "tp", None),
        P(EP, None, "tp"),
        P("tp", EP),
        P("tp", EP),
        P(EP, "tp"),
        P(),
    )
    return jax.shard_map(
        shards,
        mesh=torus,
        in_specs=placed,
        out_specs=(P(EP, "tp"), P(EP, "tp", None), P(EP, "tp", None)),
        check_vma=False,
    )
```

profile of v0, /device:TPU:1, one launch (start us, length us, event | category | flops | bytes accessed | tf_op | source)
XLA Modules:
  0.0 220.9 jit_solution(17859736883952036732)
XLA Ops:
  7.2 1.2 fusion.44
  8.4 2.1 convolution_convert_fusion.5
  12.1 1.4 fusion.70
  13.9 2.6 %convolution_add_fusion = f32[24,8,8,128]{3,2,1,0:T(8,128)} fusion(f32[24,8,8,128]{3,1,2,0:T(8,128)} %get-tuple-element.6, f32[24,8,8]{2,1,0:T(8,128)S(1)} %copy.68), kind=kOutput, calls=%fused_computation.10 | convolution fusion | flops 302202880 | bytes 1579008 | tf_op jit(solution)/shard_map/...ij,jk->...ik/dot_general | solution.py:55
  16.5 2.1 reshape.207
  18.7 3.3 %fusion.10 = bf16[24,8,64]{2,1,0:T(8,128)(2,1)S(1)} fusion(bf16[24,1,1024,64]{2,3,1,0:T(8,128)(2,1)} %param.29, f32[24,8,1024]{2,1,0:T(8,128)} %reshape.207, f32[24,8,1024]{2,1,0:T(8,128)} %copy-done.1, pred[24,1024]{1,0:T(8,128)(4,1)S(1)} %iota_compare_fusion), kind=kOutput, calls=%fused_computation.16 | convolution fusion | flops 27340800 | bytes 4767744 | tf_op jit(solution)/shard_map/bkgs,bksd->bkgd/dot_general | solution.py:71
  22.1 2.0 convolution_convert_fusion.1
  24.9 5.0 %all-to-all-start = ((bf16[4,24,2048]{2,1,0:T(8,128)(2,1)}), bf16[4,24,2048]{2,1,0:T(8,128)(2,1)S(1)}, u32[]{:S(2)}, u32[]{:S(2)}) async-start(bf16[4,24,2048]{2,1,0:T(8,128)(2,1)} %broadcast_in_dim.41), calls=%async_computation | async-start | bytes 786432 | tf_op jit(solution)/shard_map/all_to_all | solution.py:16
  29.8 6.2 %all-to-all-done = bf16[4,24,2048]{2,1,0:T(8,128)(2,1)S(1)} async-done(((bf16[4,24,2048]{2,1,0:T(8,128)(2,1)}), bf16[4,24,2048]{2,1,0:T(8,128)(2,1)S(1)}, u32[]{:S(2)}, u32[]{:S(2)}) %all-to-all-start) | async-done | bytes 393248 | tf_op jit(solution)/shard_map/all_to_all | solution.py:16
  38.0 10.2 %all-gather = bf16[96,512]{1,0:T(8,128)(2,1)S(1)} all-gather(bf16[24,512]{1,0:T(8,128)(2,1)S(1)} %constant_dynamic-slice_fusion), channel_id=2, replica_groups=mesh['ep_0'=8,'ep_1'=4,'ep_2'=2,'tp'=4] {'ep_1'}, dimensions={0}, use_global_device_ids=true | all-gather | bytes 122880 | tf_op jit(solution)/shard_map/all_gather | solution.py:33
  48.2 26.3 %all_gather.13 = bf16[32,24,512]{2,1,0:T(8,128)(2,1)} all-gather(bf16[4,24,512]{2,1,0:T(8,128)(2,1)S(1)} %bitcast.85), channel_id=1, replica_groups=mesh['ep_0'=8,'ep_1'=4,'ep_2'=2,'tp'=4] {'ep_0'}, dimensions={0}, use_global_device_ids=true | all-gather | bytes 884736 | tf_op jit(solution)/shard_map/all_gather | solution.py:33
  76.0 28.8 %all_to_all.44 = bf16[64,2,512]{2,1,0:T(2,128)(2,1)S(1)} all-to-all(bf16[64,2,512]{2,1,0:T(2,128)(2,1)S(1)} %reshape.212), channel_id=1, replica_groups=mesh['ep_0'=8,'ep_1'=4,'ep_2'=2,'tp'=4] {'ep_0','ep_1','ep_2'}, dimensions={0} | all-to-all | bytes 262144 | tf_op jit(solution)/shard_map/all_to_all | solution.py:168
  104.8 1.5 convolution_convert_fusion.2
  106.4 1.1 broadcast_in_dim.46
  107.5 4.2 %all-to-all-start.2 = ((bf16[4,128,1024]{2,1,0:T(8,128)(2,1)}), bf16[4,128,1024]{2,1,0:T(8,128)(2,1)}, u32[]{:S(2)}, u32[]{:S(2)}) async-start(bf16[4,128,1024]{2,1,0:T(8,128)(2,1)} %broadcast_in_dim.46), calls=%async_computation.2 | async-start | bytes 2097152 | tf_op jit(solution)/shard_map/all_to_all | solution.py:16
  111.8 1.7 copy.71
  113.5 1.5 convolution_convert_fusion
  115.0 11.6 %all-to-all-done.2 = bf16[4,128,1024]{2,1,0:T(8,128)(2,1)} async-done(((bf16[4,128,1024]{2,1,0:T(8,128)(2,1)}), bf16[4,128,1024]{2,1,0:T(8,128)(2,1)}, u32[]{:S(2)}, u32[]{:S(2)}) %all-to-all-start.2) | async-done | bytes 1048608 | tf_op jit(solution)/shard_map/all_to_all | solution.py:16
  126.6 3.1 %broadcast_in_dim.48 = bf16[4,1536,256]{2,1,0:T(8,128)(2,1)} broadcast(bf16[1536,256]{1,0:T(8,128)(2,1)} %convolution_convert_fusion), dimensions={1,2} | broadcast | bytes 3932160 | tf_op jit(solution)/shard_map/broadcast_in_dim | solution.py:16
  129.7 4.8 %all-to-all-start.4 = ((bf16[4,1536,256]{2,1,0:T(8,128)(2,1)}), bf16[4,1536,256]{2,1,0:T(8,128)(2,1)}, u32[]{:S(2)}, u32[]{:S(2)}) async-start(bf16[4,1536,256]{2,1,0:T(8,128)(2,1)} %broadcast_in_dim.48), calls=%async_computation.4 | async-start | bytes 6291456 | tf_op jit(solution)/shard_map/all_to_all | solution.py:16
  134.7 1.9 fusion.15
  136.5 1.8 fusion.16
  139.9 1.5 convert_reduce_fusion.1
  142.3 28.6 %all-to-all-done.4 = bf16[4,1536,256]{2,1,0:T(8,128)(2,1)} async-done(((bf16[4,1536,256]{2,1,0:T(8,128)(2,1)}), bf16[4,1536,256]{2,1,0:T(8,128)(2,1)}, u32[]{:S(2)}, u32[]{:S(2)}) %all-to-all-start.4) | async-done | bytes 3145760 | tf_op jit(solution)/shard_map/all_to_all | solution.py:16
  171.0 6.1 %all-to-all-start.3 = ((bf16[64,2,512]{2,1,0:T(2,128)(2,1)}), bf16[64,2,512]{2,1,0:T(2,128)(2,1)S(1)}, u32[]{:S(2)}, u32[]{:S(2)}) async-start(bf16[64,2,512]{2,1,0:T(2,128)(2,1)} %reshape.214), calls=%async_computation.3 | async-start | bytes 262144 | tf_op jit(solution)/shard_map/all_to_all | solution.py:177
  177.1 2.6 %convert_reduce_fusion = f32[1536,256]{1,0:T(8,128)S(1)} fusion(bf16[4,1536,256]{2,1,0:T(8,128)(2,1)} %all-to-all-done.4), kind=kLoop, calls=%fused_computation | loop fusion | flops 2752512 | bytes 4718592 | tf_op jit(solution)/shard_map/reduce_sum | solution.py:21
  180.8 7.6 %all-to-all-done.3 = bf16[64,2,512]{2,1,0:T(2,128)(2,1)S(1)} async-done(((bf16[64,2,512]{2,1,0:T(2,128)(2,1)}), bf16[64,2,512]{2,1,0:T(2,128)(2,1)S(1)}, u32[]{:S(2)}, u32[]{:S(2)}) %all-to-all-start.3) | async-done | bytes 131104 | tf_op jit(solution)/shard_map/all_to_all | solution.py:177
  189.0 4.5 %all-to-all-start.5 = ((bf16[64,24,128]{2,1,0:T(8,128)(2,1)}), bf16[64,24,128]{2,1,0:T(8,128)(2,1)S(1)}, u32[]{:S(2)}, u32[]{:S(2)}) async-start(bf16[64,24,128]{2,1,0:T(8,128)(2,1)} %bitcast.84), calls=%async_computation.5 | async-start | bytes 786432 | tf_op jit(solution)/shard_map/all_to_all | solution.py:194
  194.5 1.7 reshape.222
  196.2 1.8 convolution_reduce_fusion
  198.0 10.8 %all-to-all-done.5 = bf16[64,24,128]{2,1,0:T(8,128)(2,1)S(1)} async-done(((bf16[64,24,128]{2,1,0:T(8,128)(2,1)}), bf16[64,24,128]{2,1,0:T(8,128)(2,1)S(1)}, u32[]{:S(2)}, u32[]{:S(2)}) %all-to-all-start.5) | async-done | bytes 393248 | tf_op jit(solution)/shard_map/all_to_all | solution.py:194
  208.8 5.3 %fusion.14 = bf16[24,512]{1,0:T(8,128)(2,1)} fusion(bf16[8192,512]{1,0:T(8,128)(2,1)} %all-gather.6.cloned.1.call-done, f32[24,512]{1,0:T(8,128)} %convolution_reduce_fusion, f32[24,2048]{1,0:T(8,128)} %copy-done.2, s32[]{:T(128)S(6)} %select_n.41, f32[24]{0:T(128)S(1)} %fusion.20, bf16[64,24,128]{2,1,0:T(8,128)(2,1)S(1)} %all-to-all-done.5), kind=kOutput, calls=%fused_computation.20 | convolution fusion | flops 201375744 | bytes 8904804 | tf_op jit(solution)/shard_map/dot_general | solution.py:195
  (74 shorter events, 11.5 us)
Async XLA Ops:
  7.2 3.5 %copy-start = (bf16[24,1,1024,64]{2,3,1,0:T(8,128)(2,1)S(1)}, bf16[24,1,1024,64]{2,3,1,0:T(8,128)(2,1)}, u32[]{:S(2)}) copy-start(bf16[24,1,1024,64]{2,3,1,0:T(8,128)(2,1)} %param.28) | copy-start | bytes 9437188
  7.2 3.4 %copy-start.10 = (s32[24]{0:T(128)S(1)}, s32[24]{0:T(128)}, u32[]{:S(2)}) copy-start(s32[24]{0:T(128)} %param.30) | copy-start | bytes 292
  7.2 3.5 %copy-start.9 = (f32[8]{0:T(128)S(1)}, f32[8]{0:T(128)}, u32[]{:S(2)}) copy-start(f32[8]{0:T(128)} %param.27) | copy-start | bytes 100
  11.2 0.9 copy-start.1
  22.1 15.8 %copy-start.8 = (f32[2048]{0:T(1024)S(1)}, f32[2048]{0:T(1024)}, u32[]{:S(2)}) copy-start(f32[2048]{0:T(1024)} %param.31) | copy-start | bytes 24580
  24.9 50.4 %copy-start.6 = (s32[24,2]{0,1:T(2,128)S(1)}, s32[24,2]{0,1:T(2,128)}, u32[]{:S(2)}) copy-start(s32[24,2]{0,1:T(2,128)} %param.34) | copy-start | bytes 580
  24.9 11.2 %all-to-all-start = ((bf16[4,24,2048]{2,1,0:T(8,128)(2,1)}), bf16[4,24,2048]{2,1,0:T(8,128)(2,1)S(1)}, u32[]{:S(2)}, u32[]{:S(2)}) async-start(bf16[4,24,2048]{2,1,0:T(8,128)(2,1)} %broadcast_in_dim.41), calls=%async_computation | async-start | bytes 786432 | tf_op jit(solution)/shard_map/all_to_all | solution.py:16
  29.8 82.0 %all-gather.4.cloned.1.call-start = ((), (), s32[]{:S(2)}) async-start(), calls=%async_computation.6 | async-start | bytes 2359296 | tf_op jit(solution)/shard_map/all_gather | solution.py:33
  37.2 0.7 copy-start.2
  37.9 100.6 %copy-start.5 = (bf16[24,2048]{1,0:T(8,128)(2,1)}, bf16[24,2048]{1,0:T(8,128)(2,1)S(1)}, u32[]{:S(2)}) copy-start(bf16[24,2048]{1,0:T(8,128)(2,1)S(1)} %multiply_convert_fusion) | copy-start | bytes 294916
  74.5 134.3 %all-gather.6.cloned.1.call-start = ((), (), s32[]{:S(2)}) async-start(), calls=%async_computation.7 | async-start | bytes 8519680 | tf_op jit(solution)/shard_map/all_gather | solution.py:197
  107.5 19.1 %all-to-all-start.2 = ((bf16[4,128,1024]{2,1,0:T(8,128)(2,1)}), bf16[4,128,1024]{2,1,0:T(8,128)(2,1)}, u32[]{:S(2)}, u32[]{:S(2)}) async-start(bf16[4,128,1024]{2,1,0:T(8,128)(2,1)} %broadcast_in_dim.46), calls=%async_computation.2 | async-start | bytes 2097152 | tf_op jit(solution)/shard_map/all_to_all | solution.py:16
  111.8 1.8 copy-start.12
  111.8 1.8 copy-start.13
  129.7 5.0 %copy-start.3 = (bf16[24,2048]{1,0:T(8,128)(2,1)S(1)}, bf16[24,2048]{1,0:T(8,128)(2,1)}, u32[]{:S(2)}) copy-start(bf16[24,2048]{1,0:T(8,128)(2,1)} %param.21) | copy-start | bytes 294916
  129.7 5.0 %copy-start.7 = (f32[2048]{0:T(1024)S(1)}, f32[2048]{0:T(1024)}, u32[]{:S(2)}) copy-start(f32[2048]{0:T(1024)} %param.22) | copy-start | bytes 24580
  129.7 8.7 %copy-start.14 = (bf16[2048,4]{0,1:T(4,128)(2,1)S(1)}, bf16[2048,4]{0,1:T(4,128)(2,1)}, u32[]{:S(2)}) copy-start(bf16[2048,4]{0,1:T(4,128)(2,1)} %param.32) | copy-start | bytes 49156
  129.7 41.3 %all-to-all-start.4 = ((bf16[4,1536,256]{2,1,0:T(8,128)(2,1)}), bf16[4,1536,256]{2,1,0:T(8,128)(2,1)}, u32[]{:S(2)}, u32[]{:S(2)}) async-start(bf16[4,1536,256]{2,1,0:T(8,128)(2,1)} %broadcast_in_dim.48), calls=%async_computation.4 | async-start | bytes 6291456 | tf_op jit(solution)/shard_map/all_to_all | solution.py:16
  134.7 6.7 %copy-start.11 = (bf16[1,512,512]{2,1,0:T(8,128)(2,1)S(1)}, bf16[1,512,512]{2,1,0:T(8,128)(2,1)}, u32[]{:S(2)}) copy-start(bf16[1,512,512]{2,1,0:T(8,128)(2,1)} %param.37) | copy-start | bytes 1572868
  171.0 17.4 %all-to-all-start.3 = ((bf16[64,2,512]{2,1,0:T(2,128)(2,1)}), bf16[64,2,512]{2,1,0:T(2,128)(2,1)S(1)}, u32[]{:S(2)}, u32[]{:S(2)}) async-start(bf16[64,2,512]{2,1,0:T(2,128)(2,1)} %reshape.214), calls=%async_computation.3 | async-start | bytes 262144 | tf_op jit(solution)/shard_map/all_to_all | solution.py:177
  188.4 0.6 copy-start.4
  189.0 19.8 %all-to-all-start.5 = ((bf16[64,24,128]{2,1,0:T(8,128)(2,1)}), bf16[64,24,128]{2,1,0:T(8,128)(2,1)S(1)}, u32[]{:S(2)}, u32[]{:S(2)}) async-start(bf16[64,24,128]{2,1,0:T(8,128)(2,1)} %bitcast.84), calls=%async_computation.5 | async-start | bytes 786432 | tf_op jit(solution)/shard_map/all_to_all | solution.py:194
Sparse Core Ops, SparseCore 0:
  74.7 22.5 all-gather.3
  100.0 85.2 all-gather.5
where the time goes:
time: 222 us; the launch traced here: 221 us
  waiting for transfers between devices  65.6 us (30%)
  blocking collectives  65.4 us (29%)
  matrix products  27.1 us (12%)
  starting transfers between devices  24.6 us (11%)
  local copies, waits for them, and re-layouts  14.4 us (6%)
  between operations  14.4 us (6%)
  other arithmetic  9.43 us (4%)
    all_to_all x3, waiting for transfers between devices, copy_for_each(): lax.all_to_all(jnp.broadcast_to(x[None], (devices, *x.shape)), axis, 0, 0...  46.5 us
    all_gather x2, blocking collectives, all_blocks(): tiles = lax.all_gather(tiles, axes[k], axis=0, tiled=True)  36.5 us
    all_to_all x1, blocking collectives, shards(): lax.all_to_all(outbound, EP, split_axis=0, concat_axis=0, tiled=True)  28.8 us
    all_to_all x3, starting transfers between devices, copy_for_each(): lax.all_to_all(jnp.broadcast_to(x[None], (devices, *x.shape)), axis, 0, 0...  14 us
    all_to_all x1, waiting for transfers between devices, shards(): lax.all_to_all(dense_hidden, EP, split_axis=0, concat_axis=1, tiled=True)  10.8 us
    all_to_all x1, waiting for transfers between devices, shards(): lax.all_to_all(result.reshape(received.shape), EP, split_axis=0, concat_a...  7.59 us
    all_to_all x1, starting transfers between devices, shards(): lax.all_to_all(result.reshape(received.shape), EP, split_axis=0, concat_a...  6.15 us
    dot_general x1, matrix products, shards(): jnp.dot(own_hidden, lax.all_gather(d_down, EP, axis=0, tiled=True), prefe...  5.27 us
  transfers between devices with their start and end apart: 7, of which 5 were waited for; matrix products, arithmetic and copies ran while one was open for 12% of the time, Pallas kernels for 0%

commit v1 on v0

--- a/solution.py
+++ b/solution.py
@@ -30,7 +30,10 @@
 def all_blocks(x, axes, sequence):
     tiles = x[None]
     for k in sequence:
-        tiles = lax.all_gather(tiles, axes[k], axis=0, tiled=True)
+        devices_2 = lax.axis_size(axes[k])
+        blocks = jnp.stack([tiles for _ in range(devices_2)])
+        blocks = lax.all_to_all(blocks, axes[k], split_axis=0, concat_axis=0)
+        tiles = jnp.concatenate(blocks, axis=0)
     current = [lax.axis_size(axes[k]) for k in reversed(sequence)]
     tiles = tiles.reshape(*current, *x.shape)
     turned = sorted(range(len(sequence)), key=lambda place: sequence[len(sequence) - 1 - place])

time: 222 us -> 236 us (1.063)
  blocking collectives: 65.4 us -> 31.7 us
  waiting for transfers between devices: 65.6 us -> 96.4 us
  starting transfers between devices: 24.6 us -> 33.5 us
  local copies, waits for them, and re-layouts: 14.4 us -> 18.7 us
  other arithmetic: 9.43 us -> 13 us
    all_gather x2 -> x0, blocking collectives: 36.5 us -> none  [all_blocks(): tiles = lax.all_gather(tiles, axes[k], axis=0, tiled=True)]
    all_to_all x0 -> x2, waiting for transfers between devices: none -> 32.9 us  [all_blocks(): blocks = lax.all_to_all(blocks, axes[k], split_axis=0, concat_axis=0)]
    all_to_all x0 -> x2, starting transfers between devices: none -> 9.05 us  [all_blocks(): blocks = lax.all_to_all(blocks, axes[k], split_axis=0, concat_axis=0)]
    all_to_all x0 -> x1, blocking collectives: none -> 6.82 us  [all_blocks(): blocks = lax.all_to_all(blocks, axes[k], split_axis=0, concat_axis=0)]
    all_to_all x1, blocking collectives: 28.8 us -> 24.9 us  [shards(): lax.all_to_all(outbound, EP, split_axis=0, concat_axis=0, tiled=True)]
    another operation x1 -> x3, local copies, waits for them, and re-layouts: 0.11 us -> 2.65 us  [the longest x2 2.55 us: all_blocks(): blocks = jnp.stack([tiles for _ in range(devices_2)])]
  transfers between devices with their start and end apart: 7 -> 8, of which waited for: 5 -> 7; matrix products, arithmetic and copies ran while one was open for 12% -> 22% of each run, Pallas kernels for 0% -> 0%
where the time goes in v1:
time: 236 us; the launch traced here: 235 us
  waiting for transfers between devices  96.4 us (41%)
  starting transfers between devices  33.5 us (14%)
  blocking collectives  31.7 us (13%)
  matrix products  27.1 us (11%)
  local copies, waits for them, and re-layouts  18.7 us (8%)
  between operations  14.4 us (6%)
  other arithmetic  13 us (6%)
    all_to_all x3, waiting for transfers between devices, copy_for_each(): lax.all_to_all(jnp.broadcast_to(x[None], (devices, *x.shape)), axis, 0, 0...  44.4 us
    all_to_all x2, waiting for transfers between devices, all_blocks(): blocks = lax.all_to_all(blocks, axes[k], split_axis=0, concat_axis=0)  32.9 us
    all_to_all x1, blocking collectives, shards(): lax.all_to_all(outbound, EP, split_axis=0, concat_axis=0, tiled=True)  24.9 us
    all_to_all x3, starting transfers between devices, copy_for_each(): lax.all_to_all(jnp.broadcast_to(x[None], (devices, *x.shape)), axis, 0, 0...  13.9 us
    all_to_all x1, waiting for transfers between devices, shards(): lax.all_to_all(dense_hidden, EP, split_axis=0, concat_axis=1, tiled=True)  10.8 us
    all_to_all x2, starting transfers between devices, all_blocks(): blocks = lax.all_to_all(blocks, axes[k], split_axis=0, concat_axis=0)  9.05 us
    all_to_all x1, waiting for transfers between devices, shards(): lax.all_to_all(result.reshape(received.shape), EP, split_axis=0, concat_a...  7.67 us
    all_to_all x1, blocking collectives, all_blocks(): blocks = lax.all_to_all(blocks, axes[k], split_axis=0, concat_axis=0)  6.82 us
  transfers between devices with their start and end apart: 8, of which 7 were waited for; matrix products, arithmetic and copies ran while one was open for 22% of the time, Pallas kernels for 0%

profile of v1, /device:TPU:1, one launch (start us, length us, event | category | flops | bytes accessed | tf_op | source)
XLA Modules:
  0.0 235.0 jit_solution(7203122780323774424)
XLA Ops:
  9.7 2.1 convolution_convert_fusion.5
  15.3 2.6 %convolution_add_fusion = f32[24,8,8,128]{3,2,1,0:T(8,128)} fusion(f32[24,8,8,128]{3,1,2,0:T(8,128)} %get-tuple-element.6, f32[24,8,8]{2,1,0:T(8,128)S(1)} %copy.67), kind=kOutput, calls=%fused_computation.11 | convolution fusion | flops 302202880 | bytes 1579008 | tf_op jit(solution)/shard_map/...ij,jk->...ik/dot_general | solution.py:58
  17.9 2.1 reshape.208
  20.0 3.3 %fusion.10 = bf16[24,8,64]{2,1,0:T(8,128)(2,1)S(1)} fusion(bf16[24,1,1024,64]{2,3,1,0:T(8,128)(2,1)} %param.29, f32[24,8,1024]{2,1,0:T(8,128)} %reshape.208, f32[24,8,1024]{2,1,0:T(8,128)} %copy-done.1, pred[24,1024]{1,0:T(8,128)(4,1)S(1)} %iota_compare_fusion), kind=kOutput, calls=%fused_computation.17 | convolution fusion | flops 27340800 | bytes 4767744 | tf_op jit(solution)/shard_map/bkgs,bksd->bkgd/dot_general | solution.py:74
  23.5 2.0 convolution_convert_fusion.1
  26.3 4.8 %all-to-all-start = ((bf16[4,24,2048]{2,1,0:T(8,128)(2,1)}), bf16[4,24,2048]{2,1,0:T(8,128)(2,1)S(1)}, u32[]{:S(2)}, u32[]{:S(2)}) async-start(bf16[4,24,2048]{2,1,0:T(8,128)(2,1)} %broadcast_in_dim.35), calls=%async_computation | async-start | bytes 786432 | tf_op jit(solution)/shard_map/all_to_all | solution.py:16
  33.4 4.0 %all-to-all-done = bf16[4,24,2048]{2,1,0:T(8,128)(2,1)S(1)} async-done(((bf16[4,24,2048]{2,1,0:T(8,128)(2,1)}), bf16[4,24,2048]{2,1,0:T(8,128)(2,1)S(1)}, u32[]{:S(2)}, u32[]{:S(2)}) %all-to-all-start) | async-done | bytes 393248 | tf_op jit(solution)/shard_map/all_to_all | solution.py:16
  40.7 4.8 %all-to-all-start.4 = ((bf16[4,1,24,512]{3,2,1,0:T(8,128)(2,1)}), bf16[4,1,24,512]{3,2,1,0:T(8,128)(2,1)}, u32[]{:S(2)}, u32[]{:S(2)}) async-start(bf16[4,1,24,512]{3,2,1,0:T(8,128)(2,1)} %stack.9), calls=%async_computation.4 | async-start | bytes 196608 | tf_op jit(solution)/shard_map/all_to_all | solution.py:35
  45.8 4.5 %all-to-all-done.4 = bf16[4,1,24,512]{3,2,1,0:T(8,128)(2,1)} async-done(((bf16[4,1,24,512]{3,2,1,0:T(8,128)(2,1)}), bf16[4,1,24,512]{3,2,1,0:T(8,128)(2,1)}, u32[]{:S(2)}, u32[]{:S(2)}) %all-to-all-start.4) | async-done | bytes 98336 | tf_op jit(solution)/shard_map/all_to_all | solution.py:35
  50.3 24.9 %all_to_all.59 = bf16[64,2,512]{2,1,0:T(2,128)(2,1)S(1)} all-to-all(bf16[64,2,512]{2,1,0:T(2,128)(2,1)S(1)} %reshape.213), channel_id=1, replica_groups=mesh['ep_0'=8,'ep_1'=4,'ep_2'=2,'tp'=4] {'ep_0','ep_1','ep_2'}, dimensions={0} | all-to-all | bytes 262144 | tf_op jit(solution)/shard_map/all_to_all | solution.py:171
  75.2 1.9 stack.10
  77.1 4.2 %all-to-all-start.5 = ((bf16[8,4,24,512]{3,2,1,0:T(8,128)(2,1)}), bf16[8,4,24,512]{3,2,1,0:T(8,128)(2,1)}, u32[]{:S(2)}, u32[]{:S(2)}) async-start(bf16[8,4,24,512]{3,2,1,0:T(8,128)(2,1)} %stack.10), calls=%async_computation.5 | async-start | bytes 1572864 | tf_op jit(solution)/shard_map/all_to_all | solution.py:35
  82.1 1.6 convolution_convert_fusion.2
  83.7 28.4 %all-to-all-done.5 = bf16[8,4,24,512]{3,2,1,0:T(8,128)(2,1)} async-done(((bf16[8,4,24,512]{3,2,1,0:T(8,128)(2,1)}), bf16[8,4,24,512]{3,2,1,0:T(8,128)(2,1)}, u32[]{:S(2)}, u32[]{:S(2)}) %all-to-all-start.5) | async-done | bytes 786464 | tf_op jit(solution)/shard_map/all_to_all | solution.py:35
  112.1 1.5 pad_maximum_fusion
  113.6 6.8 %all_to_all.60 = bf16[2,32,24,512]{3,2,1,0:T(8,128)(2,1)} all-to-all(bf16[2,32,24,512]{3,2,1,0:T(8,128)(2,1)S(1)} %pad_maximum_fusion), channel_id=1, replica_groups=mesh['ep_0'=8,'ep_1'=4,'ep_2'=2,'tp'=4] {'ep_2'}, dimensions={0} | all-to-all | bytes 3145728 | tf_op jit(solution)/shard_map/all_to_all | solution.py:35
  121.5 4.3 %all-to-all-start.2 = ((bf16[4,128,1024]{2,1,0:T(8,128)(2,1)}), bf16[4,128,1024]{2,1,0:T(8,128)(2,1)}, u32[]{:S(2)}, u32[]{:S(2)}) async-start(bf16[4,128,1024]{2,1,0:T(8,128)(2,1)} %broadcast_in_dim.44), calls=%async_computation.2 | async-start | bytes 2097152 | tf_op jit(solution)/shard_map/all_to_all | solution.py:16
  125.8 1.6 copy.70
  128.9 11.8 %all-to-all-done.2 = bf16[4,128,1024]{2,1,0:T(8,128)(2,1)} async-done(((bf16[4,128,1024]{2,1,0:T(8,128)(2,1)}), bf16[4,128,1024]{2,1,0:T(8,128)(2,1)}, u32[]{:S(2)}, u32[]{:S(2)}) %all-to-all-start.2) | async-done | bytes 1048608 | tf_op jit(solution)/shard_map/all_to_all | solution.py:16
  140.7 3.1 %broadcast_in_dim.45 = bf16[4,1536,256]{2,1,0:T(8,128)(2,1)} broadcast(bf16[1536,256]{1,0:T(8,128)(2,1)} %convolution_convert_fusion), dimensions={1,2} | broadcast | bytes 3932160 | tf_op jit(solution)/shard_map/broadcast_in_dim | solution.py:16
  143.8 4.8 %all-to-all-start.7 = ((bf16[4,1536,256]{2,1,0:T(8,128)(2,1)}), bf16[4,1536,256]{2,1,0:T(8,128)(2,1)}, u32[]{:S(2)}, u32[]{:S(2)}) async-start(bf16[4,1536,256]{2,1,0:T(8,128)(2,1)} %broadcast_in_dim.45), calls=%async_computation.7 | async-start | bytes 6291456 | tf_op jit(solution)/shard_map/all_to_all | solution.py:16
  148.8 1.9 fusion.15
  150.6 1.8 fusion.16
  156.4 28.6 %all-to-all-done.7 = bf16[4,1536,256]{2,1,0:T(8,128)(2,1)} async-done(((bf16[4,1536,256]{2,1,0:T(8,128)(2,1)}), bf16[4,1536,256]{2,1,0:T(8,128)(2,1)}, u32[]{:S(2)}, u32[]{:S(2)}) %all-to-all-start.7) | async-done | bytes 3145760 | tf_op jit(solution)/shard_map/all_to_all | solution.py:16
  185.1 6.1 %all-to-all-start.3 = ((bf16[64,2,512]{2,1,0:T(2,128)(2,1)}), bf16[64,2,512]{2,1,0:T(2,128)(2,1)S(1)}, u32[]{:S(2)}, u32[]{:S(2)}) async-start(bf16[64,2,512]{2,1,0:T(2,128)(2,1)} %reshape.215), calls=%async_computation.3 | async-start | bytes 262144 | tf_op jit(solution)/shard_map/all_to_all | solution.py:180
  191.2 2.5 %convert_reduce_fusion = f32[1536,256]{1,0:T(8,128)S(1)} fusion(bf16[4,1536,256]{2,1,0:T(8,128)(2,1)} %all-to-all-done.7), kind=kLoop, calls=%fused_computation | loop fusion | flops 2752512 | bytes 4718592 | tf_op jit(solution)/shard_map/reduce_sum | solution.py:21
  194.8 7.7 %all-to-all-done.3 = bf16[64,2,512]{2,1,0:T(2,128)(2,1)S(1)} async-done(((bf16[64,2,512]{2,1,0:T(2,128)(2,1)}), bf16[64,2,512]{2,1,0:T(2,128)(2,1)S(1)}, u32[]{:S(2)}, u32[]{:S(2)}) %all-to-all-start.3) | async-done | bytes 131104 | tf_op jit(solution)/shard_map/all_to_all | solution.py:180
  203.1 4.5 %all-to-all-start.8 = ((bf16[64,24,128]{2,1,0:T(8,128)(2,1)}), bf16[64,24,128]{2,1,0:T(8,128)(2,1)S(1)}, u32[]{:S(2)}, u32[]{:S(2)}) async-start(bf16[64,24,128]{2,1,0:T(8,128)(2,1)} %bitcast.85), calls=%async_computation.8 | async-start | bytes 786432 | tf_op jit(solution)/shard_map/all_to_all | solution.py:197
  208.6 1.7 reshape.221
  210.3 1.8 convolution_reduce_fusion
  212.1 10.8 %all-to-all-done.8 = bf16[64,24,128]{2,1,0:T(8,128)(2,1)S(1)} async-done(((bf16[64,24,128]{2,1,0:T(8,128)(2,1)}), bf16[64,24,128]{2,1,0:T(8,128)(2,1)S(1)}, u32[]{:S(2)}, u32[]{:S(2)}) %all-to-all-start.8) | async-done | bytes 393248 | tf_op jit(solution)/shard_map/all_to_all | solution.py:197
  222.9 5.3 %fusion.14 = bf16[24,512]{1,0:T(8,128)(2,1)} fusion(bf16[8192,512]{1,0:T(8,128)(2,1)} %all-gather.2.cloned.1.call-done, f32[24,512]{1,0:T(8,128)} %convolution_reduce_fusion, f32[24,2048]{1,0:T(8,128)} %copy-done.2, s32[]{:T(128)S(6)} %select_n.41, f32[24]{0:T(128)S(1)} %fusion.20, bf16[64,24,128]{2,1,0:T(8,128)(2,1)S(1)} %all-to-all-done.8), kind=kOutput, calls=%fused_computation.21 | convolution fusion | flops 201375744 | bytes 8904804 | tf_op jit(solution)/shard_map/dot_general | solution.py:198
  (83 shorter events, 22.8 us)
Async XLA Ops:
  7.2 4.8 %copy-start = (bf16[24,1,1024,64]{2,3,1,0:T(8,128)(2,1)S(1)}, bf16[24,1,1024,64]{2,3,1,0:T(8,128)(2,1)}, u32[]{:S(2)}) copy-start(bf16[24,1,1024,64]{2,3,1,0:T(8,128)(2,1)} %param.28) | copy-start | bytes 9437188
  7.2 4.7 %copy-start.11 = (s32[24]{0:T(128)S(1)}, s32[24]{0:T(128)}, u32[]{:S(2)}) copy-start(s32[24]{0:T(128)} %param.30) | copy-start | bytes 292
  7.2 4.8 %copy-start.8 = (f32[8]{0:T(128)S(1)}, f32[8]{0:T(128)}, u32[]{:S(2)}) copy-start(f32[8]{0:T(128)} %param.27) | copy-start | bytes 100
  7.2 215.7 %all-gather.2.cloned.1.call-start = ((), (), s32[]{:S(2)}) async-start(), calls=%async_computation.9 | async-start | bytes 8519680 | tf_op jit(solution)/shard_map/all_gather | solution.py:200
  9.2 0.5 copy-start.9
  12.5 0.9 copy-start.1
  23.3 7.8 %copy-start.6 = (s32[24,2]{0,1:T(2,128)S(1)}, s32[24,2]{0,1:T(2,128)}, u32[]{:S(2)}) copy-start(s32[24,2]{0,1:T(2,128)} %param.34) | copy-start | bytes 580
  26.3 11.1 %all-to-all-start = ((bf16[4,24,2048]{2,1,0:T(8,128)(2,1)}), bf16[4,24,2048]{2,1,0:T(8,128)(2,1)S(1)}, u32[]{:S(2)}, u32[]{:S(2)}) async-start(bf16[4,24,2048]{2,1,0:T(8,128)(2,1)} %broadcast_in_dim.35), calls=%async_computation | async-start | bytes 786432 | tf_op jit(solution)/shard_map/all_to_all | solution.py:16
  32.7 4.7 %copy-start.12 = (s32[48]{0:T(128)}, s32[48]{0:T(128)S(1)}, u32[]{:S(2)}) copy-start(s32[48]{0:T(128)S(1)} %convert_reduce_fusion.3) | copy-start | bytes 580
  38.5 0.7 copy-start.2
  40.0 112.7 %copy-start.5 = (bf16[24,2048]{1,0:T(8,128)(2,1)}, bf16[24,2048]{1,0:T(8,128)(2,1)S(1)}, u32[]{:S(2)}) copy-start(bf16[24,2048]{1,0:T(8,128)(2,1)S(1)} %multiply_convert_fusion) | copy-start | bytes 294916
  40.7 9.6 %all-to-all-start.4 = ((bf16[4,1,24,512]{3,2,1,0:T(8,128)(2,1)}), bf16[4,1,24,512]{3,2,1,0:T(8,128)(2,1)}, u32[]{:S(2)}, u32[]{:S(2)}) async-start(bf16[4,1,24,512]{3,2,1,0:T(8,128)(2,1)} %stack.9), calls=%async_computation.4 | async-start | bytes 196608 | tf_op jit(solution)/shard_map/all_to_all | solution.py:35
  77.1 34.9 %all-to-all-start.5 = ((bf16[8,4,24,512]{3,2,1,0:T(8,128)(2,1)}), bf16[8,4,24,512]{3,2,1,0:T(8,128)(2,1)}, u32[]{:S(2)}, u32[]{:S(2)}) async-start(bf16[8,4,24,512]{3,2,1,0:T(8,128)(2,1)} %stack.10), calls=%async_computation.5 | async-start | bytes 1572864 | tf_op jit(solution)/shard_map/all_to_all | solution.py:35
  121.5 19.1 %all-to-all-start.2 = ((bf16[4,128,1024]{2,1,0:T(8,128)(2,1)}), bf16[4,128,1024]{2,1,0:T(8,128)(2,1)}, u32[]{:S(2)}, u32[]{:S(2)}) async-start(bf16[4,128,1024]{2,1,0:T(8,128)(2,1)} %broadcast_in_dim.44), calls=%async_computation.2 | async-start | bytes 2097152 | tf_op jit(solution)/shard_map/all_to_all | solution.py:16
  125.8 1.7 copy-start.15
  125.8 1.7 copy-start.16
  143.8 4.8 %copy-start.13 = (s32[48]{0:T(128)S(1)}, s32[48]{0:T(128)}, u32[]{:S(2)}) copy-start(s32[48]{0:T(128)} %copy-done.12) | copy-start | bytes 580
  143.8 5.0 %copy-start.3 = (bf16[24,2048]{1,0:T(8,128)(2,1)S(1)}, bf16[24,2048]{1,0:T(8,128)(2,1)}, u32[]{:S(2)}) copy-start(bf16[24,2048]{1,0:T(8,128)(2,1)} %param.21) | copy-start | bytes 294916
  143.8 5.0 %copy-start.7 = (f32[2048]{0:T(1024)S(1)}, f32[2048]{0:T(1024)}, u32[]{:S(2)}) copy-start(f32[2048]{0:T(1024)} %param.22) | copy-start | bytes 24580
  143.8 5.0 %copy-start.10 = (f32[24]{0:T(128)S(1)}, f32[24]{0:T(128)}, u32[]{:S(2)}) copy-start(f32[24]{0:T(128)} %copy-done.9) | copy-start | bytes 292
  143.8 8.7 %copy-start.17 = (bf16[2048,4]{0,1:T(4,128)(2,1)S(1)}, bf16[2048,4]{0,1:T(4,128)(2,1)}, u32[]{:S(2)}) copy-start(bf16[2048,4]{0,1:T(4,128)(2,1)} %param.32) | copy-start | bytes 49156
  143.8 41.3 %all-to-all-start.7 = ((bf16[4,1536,256]{2,1,0:T(8,128)(2,1)}), bf16[4,1536,256]{2,1,0:T(8,128)(2,1)}, u32[]{:S(2)}, u32[]{:S(2)}) async-start(bf16[4,1536,256]{2,1,0:T(8,128)(2,1)} %broadcast_in_dim.45), calls=%async_computation.7 | async-start | bytes 6291456 | tf_op jit(solution)/shard_map/all_to_all | solution.py:16
  148.8 6.7 %copy-start.14 = (bf16[1,512,512]{2,1,0:T(8,128)(2,1)S(1)}, bf16[1,512,512]{2,1,0:T(8,128)(2,1)}, u32[]{:S(2)}) copy-start(bf16[1,512,512]{2,1,0:T(8,128)(2,1)} %param.37) | copy-start | bytes 1572868
  185.1 17.4 %all-to-all-start.3 = ((bf16[64,2,512]{2,1,0:T(2,128)(2,1)}), bf16[64,2,512]{2,1,0:T(2,128)(2,1)S(1)}, u32[]{:S(2)}, u32[]{:S(2)}) async-start(bf16[64,2,512]{2,1,0:T(2,128)(2,1)} %reshape.215), calls=%async_computation.3 | async-start | bytes 262144 | tf_op jit(solution)/shard_map/all_to_all | solution.py:180
  202.4 0.7 copy-start.4
  203.1 19.8 %all-to-all-start.8 = ((bf16[64,24,128]{2,1,0:T(8,128)(2,1)}), bf16[64,24,128]{2,1,0:T(8,128)(2,1)S(1)}, u32[]{:S(2)}, u32[]{:S(2)}) async-start(bf16[64,24,128]{2,1,0:T(8,128)(2,1)} %bitcast.85), calls=%async_computation.8 | async-start | bytes 786432 | tf_op jit(solution)/shard_map/all_to_all | solution.py:197
Sparse Core Ops, SparseCore 0:
  10.8 100.6 all-gather.1
